TPU v7x, 32 devices: a whole 2x2x4 slice. The times are simulated.
32 devices in a mesh: sp: 16 (over z, x, core), tp: 2 (over y).
Axes of the slice: x: 2, y: 2, z: 4, core: 2. Of those that a mesh axis runs over, the one named last changes fastest.
Arguments:
- stream: bfloat16 [2048, 16384], P('tp', 'sp'), may hold values from -12 to 12
- norm_gain: float32 [2, 2048], P(None, 'tp'), may hold values from 0.1 to 1.9
- in_weight: bfloat16 [2, 2048, 1024], P(None, 'sp', 'tp'), may hold values from -0.125 to 0.125
- out_weight: bfloat16 [2, 1024, 2048], P(None, 'tp', 'sp'), may hold values from -0.1875 to 0.1875
- docs: int32 [16384], P('sp'), may hold values from 0 to 3, never falling along the last dimension, each value on 1 to 8192 neighbouring positions
Outputs:
- mixed_out: bfloat16 [2048, 16384], P('tp', 'sp')
Inputs may be any that keep to these rules, and one draw needn't show every extreme that they name: `docs`: numbers never fall along the positions and start at 0; a document spans at most 8192 positions.
All inputs are finite; a program needn't handle non-finite values.
Results may differ from a plain program's by a relative error of at most 0.0095.
Values may be sent and summed in bfloat16 or wider, within the bound.
No kernel may reach another device: no remote copies, remote signals or barrier semaphores. Data moves between devices by JAX's collectives and lax.ppermute only.
A program may use at most 64 MiB of HBM per device.

v0:
```python
import jax
import jax.numpy as jnp
from jax import lax
from jax.sharding import PartitionSpec as P

D = 2048
PW = 1024
GROUPS = 4
WIDEST = 16
LAYERS = 2


contract_rows = (((0,), (0,)), ((), ()))


def passed_along(block, axis, distance):
    devices = range(lax.axis_size(axis))
    route = [(i - distance, i) for i in devices if i - distance in devices]
    return lax.ppermute(block, axis, route)


def trailing_pool(values, docs_own, edge_values, edge_docs, widths):
    length = values.shape[1]
    reach_back = WIDEST - 1
    extended = jnp.concatenate([edge_values, values], axis=1).astype(jnp.float32)
    ext_docs = jnp.concatenate([edge_docs, docs_own + 1])
    marker = docs_own + 1
    window_sum = jnp.zeros(values.shape, jnp.float32)
    members = jnp.zeros(values.shape, jnp.float32)
    for lag_step in range(WIDEST):
        lower_edge = reach_back - lag_step
        shifted = lax.slice_in_dim(extended, lower_edge, lower_edge + length, axis=1)
        same_doc = lax.slice_in_dim(ext_docs, lower_edge, lower_edge + length) == marker
        inside = jnp.logical_and(same_doc[None, :], lag_step < widths[:, None])
        window_sum = window_sum + jnp.where(inside, shifted, jnp.float32(0.0))
        members = members + inside.astype(jnp.float32)
    return (window_sum / members - values.astype(jnp.float32)).astype(jnp.bfloat16)


def per_device(stream, norm_gain, in_weight, out_weight, docs):
    local_rows, length = stream.shape
    pool_rows = in_weight.shape[2]
    channel = lax.axis_index("tp") * pool_rows + lax.iota(jnp.int32, pool_rows)
    widths = jnp.left_shift(jnp.int32(2), channel // (PW // GROUPS))
    residual = stream.astype(jnp.float32)
    for layer_idx in range(LAYERS):
        in_block, out_rows = (
            lax.all_gather(in_weight[layer_idx], "sp", axis=0, tiled=True),
            lax.all_gather(out_weight[layer_idx], "sp", axis=1, tiled=True),
        )
        squares = lax.psum(jnp.sum(residual * residual, axis=0), "tp")
        scaled = residual * lax.rsqrt(squares / D + 1e-06)[None, :] * norm_gain[layer_idx][:, None]
        normed = scaled.astype(jnp.bfloat16)
        pool_in = lax.dot_general(
            in_block,
            lax.all_gather(normed, "tp", axis=0, tiled=True),
            contract_rows,
            preferred_element_type=jnp.float32,
        ).astype(jnp.bfloat16)
        tail_from = length - WIDEST + 1
        edge_values, edge_docs = passed_along(
            (pool_in[:, tail_from:], docs[tail_from:] + 1), "sp", 1
        )
        pooled = trailing_pool(pool_in, docs, edge_values, edge_docs, widths)
        out_cols = lax.all_to_all(out_rows, "tp", split_axis=1, concat_axis=0, tiled=True)
        change = lax.dot_general(
            out_cols,
            lax.all_gather(pooled, "tp", axis=0, tiled=True),
            contract_rows,
            preferred_element_type=jnp.float32,
        )
        residual = residual + change
    return residual.astype(jnp.bfloat16)


def solution(mesh):
    return jax.shard_map(
        per_device,
        mesh=mesh,
        in_specs=(P("tp", "sp"), P(None, "tp"), P(None, "sp", "tp"), P(None, "tp", "sp"), P("sp")),
        out_specs=P("tp", "sp"),
        check_vma=False,
    )
```

profile of v0, /device:TPU:0, one launch (start us, length us, event | category | flops | bytes accessed | tf_op | source)
XLA Modules:
  0.0 416.0 jit_solution(8553323863351046496)
XLA Ops:
  6.5 1.8 fusion.102
  8.4 0.0 all-gather.13.cloned.1.call-start
  8.5 2.1 fusion
  10.5 5.9 %psum.14 = f32[1024]{0:T(1024)S(1)} all-reduce(f32[1024]{0:T(1024)S(1)} %fusion), channel_id=1, replica_groups=mesh['sp'=16,'tp'=2] {'tp'}, use_global_device_ids=true, to_apply=%region_1.2 | all-reduce | flops 1024 | bytes 8192 | tf_op jit(solution)/shard_map/psum | solution.py:51
  16.5 1.8 fusion.2
  18.3 0.0 all-gather.23.cloned.1.call-start
  18.4 0.6 copy-done.3
  19.0 0.1 slice_add_fusion
  19.1 1.3 collective-permute-start.1
  20.4 0.8 copy.14
  21.2 0.0 all-gather.23.cloned.1.call-update
  21.2 0.0 all-gather.15.cloned.1.call-start
  21.4 0.1 fusion.70
  21.5 32.2 %all-gather.21.cloned.1.call-done = bf16[1,2048,512]{2,1,0:T(8,128)(2,1)} async-done(((bf16[1,128,512]{2,1,0:T(8,128)(2,1)}), bf16[1,2048,512]{2,1,0:T(8,128)(2,1)}) %all-gather.21.cloned.1.call-update) | async-done | bytes 2097168 | tf_op jit(solution)/shard_map/all_gather | solution.py:48
  53.7 57.0 %all-gather.13.cloned.1.call-done = bf16[2048,1024]{1,0:T(8,128)(2,1)} async-done(((bf16[1024,1024]{1,0:T(8,128)(2,1)}), bf16[2048,1024]{1,0:T(8,128)(2,1)}) %all-gather.13.cloned.1.call-update) | async-done | bytes 4194320 | tf_op jit(solution)/shard_map/all_gather | solution.py:56
  110.7 5.2 %fusion.64 = bf16[512,1024]{0,1:T(8,128)(2,1)S(1)} fusion(bf16[2048,1024]{1,0:T(8,128)(2,1)} %all-gather.13.cloned.1.call-done, bf16[1,2048,512]{2,1,0:T(8,128)(2,1)} %all-gather.21.cloned.1.call-done), kind=kOutput, calls=%fused_computation.113 | convolution fusion | flops 2148007936 | bytes 7340032 | tf_op jit(solution)/shard_map/dot_general | solution.py:54
  116.0 1.6 collective-permute-start
  117.6 0.1 fusion.72
  117.7 0.7 collective-permute-done
  118.4 0.3 maximum_convert_fusion
  118.7 10.4 %subtract_convert_fusion.1 = bf16[512,1024]{0,1:T(8,128)(2,1)} fusion(bf16[512,1024]{0,1:T(8,128)(2,1)S(1)} %fusion.64, f32[512,1039]{0,1:T(8,128)S(1)} %maximum_convert_fusion, pred[512]{0:T(512)(128)(4,1)S(1)} %get-tuple-element.28, pred[512]{0:T(512)(128)(4,1)S(1)} %get-tuple-element.29, pred[512]{0:T(512)(128)(4,1)S(1)} %get-tuple-element.30, ...), kind=kLoop, calls=%fused_computation.109 | loop fusion | flops 41943040 | bytes 35677184 | tf_op jit(solution)/shard_map/convert_element_type | solution.py:37
  129.1 0.0 all-gather.15.cloned.1.call-update
  129.1 0.0 all-gather.25.cloned.1.call-start
  129.2 0.5 all-gather.25.cloned.1.call-update
  129.7 0.0 all-gather.17.cloned.1.call-start
  129.7 24.6 %all-gather.23.cloned.1.call-done = bf16[1,512,2048]{1,2,0:T(8,128)(2,1)} async-done(((bf16[1,512,128]{1,2,0:T(8,128)(2,1)}), bf16[1,512,2048]{1,2,0:T(8,128)(2,1)}) %all-gather.23.cloned.1.call-update) | async-done | bytes 2097168 | tf_op jit(solution)/shard_map/all_gather | solution.py:49
  154.4 52.4 %all_to_all.38 = bf16[512,2,1024]{0,2,1:T(8,128)(2,1)} all-to-all(bf16[512,2,1024]{0,2,1:T(8,128)(2,1)} %bitcast.40), channel_id=1, replica_groups=mesh['sp'=16,'tp'=2] {'tp'}, dimensions={1} | all-to-all | bytes 4194304 | tf_op jit(solution)/shard_map/all_to_all | solution.py:65
  206.8 3.9 copy.9
  210.7 6.8 %multiply_reduce_fusion = (f32[1024]{0:T(1024)S(1)}, f32[1024,1024]{1,0:T(8,128)}) fusion(bf16[1024,1024]{0,1:T(8,128)(2,1)} %all-gather.15.cloned.1.call-done, bf16[1024,1024]{1,0:T(8,128)(2,1)} %bitcast.42, bf16[1024,1024]{1,0:T(8,128)(2,1)S(1)} %copy-done), kind=kOutput, calls=%fused_computation.9 | convolution fusion | flops 2151676928 | bytes 10489856 | tf_op jit(solution)/shard_map/dot_general | solution.py:66
  217.5 4.9 %psum.15 = f32[1024]{0:T(1024)S(1)} all-reduce(f32[1024]{0:T(1024)S(1)} %get-tuple-element.26), channel_id=1, replica_groups=mesh['sp'=16,'tp'=2] {'tp'}, use_global_device_ids=true, to_apply=%region_3.4 | all-reduce | flops 1024 | bytes 8192 | tf_op jit(solution)/shard_map/psum | solution.py:51
  222.4 3.9 multiply_convert_fusion
  226.3 0.0 all-gather.17.cloned.1.call-update
  226.3 0.0 all-gather.27.cloned.1.call-start
  226.4 0.8 copy.15
  227.1 0.0 all-gather.27.cloned.1.call-update
  227.2 0.0 all-gather.19.cloned.1.call-start
  227.2 22.3 %all-gather.25.cloned.1.call-done = bf16[1,2048,512]{2,1,0:T(8,128)(2,1)} async-done(((bf16[1,128,512]{2,1,0:T(8,128)(2,1)}), bf16[1,2048,512]{2,1,0:T(8,128)(2,1)}) %all-gather.25.cloned.1.call-update) | async-done | bytes 2097168 | tf_op jit(solution)/shard_map/all_gather | solution.py:48
  249.5 56.9 %all-gather.17.cloned.1.call-done = bf16[2048,1024]{1,0:T(8,128)(2,1)} async-done(((bf16[1024,1024]{1,0:T(8,128)(2,1)}), bf16[2048,1024]{1,0:T(8,128)(2,1)}) %all-gather.17.cloned.1.call-update) | async-done | bytes 4194320 | tf_op jit(solution)/shard_map/all_gather | solution.py:56
  306.4 5.2 %fusion.61 = bf16[512,1024]{0,1:T(8,128)(2,1)S(1)} fusion(bf16[2048,1024]{1,0:T(8,128)(2,1)} %all-gather.17.cloned.1.call-done, bf16[1,2048,512]{2,1,0:T(8,128)(2,1)} %all-gather.25.cloned.1.call-done), kind=kOutput, calls=%fused_computation.112 | convolution fusion | flops 2148007936 | bytes 7340032 | tf_op jit(solution)/shard_map/dot_general | solution.py:54
  311.6 1.8 collective-permute-start.2
  313.4 0.6 collective-permute-done.2
  314.0 0.3 maximum_convert_fusion.1
  314.3 10.4 %subtract_convert_fusion = bf16[512,1024]{0,1:T(8,128)(2,1)} fusion(bf16[512,1024]{0,1:T(8,128)(2,1)S(1)} %fusion.61, f32[512,1039]{0,1:T(8,128)S(1)} %maximum_convert_fusion.1, pred[512]{0:T(512)(128)(4,1)S(1)} %get-tuple-element.28, pred[512]{0:T(512)(128)(4,1)S(1)} %get-tuple-element.29, pred[512]{0:T(512)(128)(4,1)S(1)} %get-tuple-element.30, ...), kind=kLoop, calls=%fused_computation.108 | loop fusion | flops 41943040 | bytes 35677184 | tf_op jit(solution)/shard_map/convert_element_type | solution.py:37
  324.7 25.3 %all-gather.27.cloned.1.call-done = bf16[1,512,2048]{1,2,0:T(8,128)(2,1)} async-done(((bf16[1,512,128]{1,2,0:T(8,128)(2,1)}), bf16[1,512,2048]{1,2,0:T(8,128)(2,1)}) %all-gather.27.cloned.1.call-update) | async-done | bytes 2097168 | tf_op jit(solution)/shard_map/all_gather | solution.py:49
  350.0 48.5 %all_to_all.39 = bf16[512,2,1024]{0,2,1:T(8,128)(2,1)S(1)} all-to-all(bf16[512,2,1024]{0,2,1:T(8,128)(2,1)} %bitcast.41), channel_id=1, replica_groups=mesh['sp'=16,'tp'=2] {'tp'}, dimensions={1} | all-to-all | bytes 4194304 | tf_op jit(solution)/shard_map/all_to_all | solution.py:65
  398.5 2.5 copy.11
  401.0 1.0 all-gather.19.cloned.1.call-done
  402.0 7.2 %fusion.3 = bf16[1024,1024]{1,0:T(8,128)(2,1)} fusion(f32[1024,1024]{1,0:T(8,128)} %get-tuple-element.27, bf16[1024,1024]{0,1:T(8,128)(2,1)} %all-gather.19.cloned.1.call-done, bf16[1024,1024]{1,0:T(8,128)(2,1)} %bitcast.43), kind=kOutput, calls=%fused_computation.7 | convolution fusion | flops 2149580800 | bytes 10485760 | tf_op jit(solution)/shard_map/dot_general | solution.py:66
  (29 shorter events, 0.3 us)
Async XLA Ops:
  6.5 9.9 %copy-start = (bf16[1024,1024]{1,0:T(8,128)(2,1)S(1)}, bf16[1024,1024]{1,0:T(8,128)(2,1)}, u32[]{:S(2)}) copy-start(bf16[1024,1024]{1,0:T(8,128)(2,1)} %param.5) | copy-start | bytes 6291460
  6.5 9.9 %copy-start.2 = (f32[2,1024]{1,0:T(2,128)S(1)}, f32[2,1024]{1,0:T(2,128)}, u32[]{:S(2)}) copy-start(f32[2,1024]{1,0:T(2,128)} %param.6) | copy-start | bytes 24580
  6.5 47.2 %all-gather.21.cloned.1.call-start = ((), (), s32[]{:S(2)}) async-start(), calls=%async_computation.6 | async-start | bytes 2228224 | tf_op jit(solution)/shard_map/all_gather | solution.py:48
  8.4 102.3 %all-gather.13.cloned.1.call-start = ((), (), s32[]{:S(2)}) async-start(), calls=%async_computation.2 | async-start | bytes 6291456 | tf_op jit(solution)/shard_map/all_gather | solution.py:56
  18.3 0.7 copy-start.3
  18.3 2.0 copy-start.1
  18.3 136.1 %all-gather.23.cloned.1.call-start = ((), (), s32[]{:S(2)}) async-start(), calls=%async_computation.7 | async-start | bytes 2228224 | tf_op jit(solution)/shard_map/all_gather | solution.py:49
  19.1 2.4 collective-permute-start.1
  21.2 189.5 %all-gather.15.cloned.1.call-start = ((), (), s32[]{:S(2)}) async-start(), calls=%async_computation.3 | async-start | bytes 3145728 | tf_op jit(solution)/shard_map/all_gather | solution.py:68
  116.0 2.4 collective-permute-start
  129.1 120.4 %all-gather.25.cloned.1.call-start = ((), (), s32[]{:S(2)}) async-start(), calls=%async_computation.8 | async-start | bytes 2228224 | tf_op jit(solution)/shard_map/all_gather | solution.py:48
  129.7 176.7 %all-gather.17.cloned.1.call-start = ((), (), s32[]{:S(2)}) async-start(), calls=%async_computation.4 | async-start | bytes 6291456 | tf_op jit(solution)/shard_map/all_gather | solution.py:56
  226.3 123.7 %all-gather.27.cloned.1.call-start = ((), (), s32[]{:S(2)}) async-start(), calls=%async_computation.9 | async-start | bytes 2228224 | tf_op jit(solution)/shard_map/all_gather | solution.py:49
  227.2 174.8 %all-gather.19.cloned.1.call-start = ((), (), s32[]{:S(2)}) async-start(), calls=%async_computation.5 | async-start | bytes 3145728 | tf_op jit(solution)/shard_map/all_gather | solution.py:68
  311.6 2.4 collective-permute-start.2
Sparse Core Ops, SparseCore 0:
  9.5 44.1 all-gather.20
  55.2 55.4 all-gather.12
  112.9 41.4 all-gather.22
  155.8 52.3 all-gather.14
  210.2 39.2 all-gather.24
  250.9 55.4 all-gather.16
  308.5 41.4 all-gather.26
  351.5 50.3 all-gather.18
where the time goes:
time: 417 us; the launch traced here: 416 us
  waiting for transfers between devices  221 us (53%)
  blocking collectives  112 us (27%)
  other arithmetic  29.6 us (7%)
  matrix products  24.4 us (6%)
  between operations  13.7 us (3%)
  local copies, waits for them, and re-layouts  10.5 us (3%)
  starting transfers between devices  4.9 us (1%)
    all_gather x2, waiting for transfers between devices, per_device(): lax.all_gather(normed, 'tp', axis=0, tiled=True)  114 us
    all_to_all x2, blocking collectives, per_device(): lax.all_to_all(out_rows, 'tp', split_axis=1, concat_axis=0, tiled=True)  101 us
    all_gather x2, waiting for transfers between devices, per_device(): lax.all_gather(in_weight[layer_idx], 'sp', axis=0, tiled=True)  54.4 us
    all_gather x2, waiting for transfers between devices, per_device(): lax.all_gather(out_weight[layer_idx], 'sp', axis=1, tiled=True)  49.9 us
    convert_element_type x2, other arithmetic, trailing_pool(): (window_sum / members - values.astype(jnp.float32)).astype(jnp.bfloat16)  20.8 us
    dot_general x2, matrix products, per_device(): lax.dot_general(out_cols, lax.all_gather(pooled, 'tp', axis=0, tiled=True...  13.9 us
    psum x2, blocking collectives, per_device(): squares = lax.psum(jnp.sum(residual * residual, axis=0), 'tp')  10.8 us
    dot_general x2, matrix products, per_device(): lax.dot_general(in_block, lax.all_gather(normed, 'tp', axis=0, tiled=True...  10.4 us
  transfers between devices with their start and end apart: 11, of which 9 were waited for; matrix products, arithmetic and copies ran while one was open for 13% of the time, Pallas kernels for 0%

commit v1 on v0

--- a/solution.py
+++ b/solution.py
@@ -1,6 +1,10 @@
+import functools
+
 import jax
 import jax.numpy as jnp
 from jax import lax
+from jax.experimental import pallas as pl
+from jax.experimental.pallas import tpu as pltpu
 from jax.sharding import PartitionSpec as P
 
 D = 2048
@@ -8,7 +12,8 @@
 GROUPS = 4
 WIDEST = 16
 LAYERS = 2
-
+HALO = 128
+BOTH = ("sp", "tp")
 
 contract_rows = (((0,), (0,)), ((), ()))
 
@@ -37,7 +42,7 @@
     return (window_sum / members - values.astype(jnp.float32)).astype(jnp.bfloat16)
 
 
-def per_device(stream, norm_gain, in_weight, out_weight, docs):
+def split_channels(stream, norm_gain, in_weight, out_weight, docs):
     local_rows, length = stream.shape
     pool_rows = in_weight.shape[2]
     channel = lax.axis_index("tp") * pool_rows + lax.iota(jnp.int32, pool_rows)
@@ -73,6 +78,132 @@
     return residual.astype(jnp.bfloat16)
 
 
+def pieces_at(ids, pieces, target, sems, place):
+    copies, k = [], 0
+    for ref in pieces:
+        for n in range(ref.shape[0]):
+            copies.append(pltpu.make_async_copy(ref.at[n], place(target, ids[0, k], ids[1, k]), sems.at[k]))
+            k += 1
+    return copies
+
+
+def in_kernel(ids, x_ref, gain_ref, docs_ref, *rest, parts, layer_first):
+    pieces, (pooled_ref, w_buf, sems) = rest[:parts], rest[parts:]
+    rows, cols = pieces[0].shape[1:]
+    place = lambda target, i, j: target.at[pl.ds(pl.multiple_of(i * rows, rows), rows),
+                                           pl.ds(pl.multiple_of(j * cols, cols), cols)]
+    copies = pieces_at(ids, pieces, w_buf, sems, place)
+    for copy in copies:
+        copy.start()
+    x = x_ref[...].astype(jnp.float32)
+    mean_square = jnp.sum(x * x, axis=0, keepdims=True) / x.shape[0]
+    normed = (x * lax.rsqrt(mean_square + 1e-06) * gain_ref[...]).astype(jnp.bfloat16)
+    docs = docs_ref[...]
+    wide = PW // GROUPS
+    for copy in copies:
+        copy.wait()
+    same, members = {}, {}
+    count = jnp.ones(docs.shape, jnp.float32)
+    lag = 1
+    for group in range(GROUPS):
+        same[lag] = pltpu.roll(docs, lag, 1) == docs
+        count = count + jnp.where(same[lag], pltpu.roll(count, lag, 1), 0.0)
+        members[group] = 1.0 / count
+        lag *= 2
+    for group in range(GROUPS):
+        chans = slice(group * wide, (group + 1) * wide)
+        value = lax.dot_general(w_buf[:, chans], normed, contract_rows, preferred_element_type=jnp.float32)
+        value = value.astype(jnp.bfloat16).astype(jnp.float32)
+        total, lag = value, 1
+        for _ in range(group + 1):
+            total = total + jnp.where(same[lag], pltpu.roll(total, lag, 1), 0.0)
+            lag *= 2
+        pooled_ref[chans, :] = (total * members[group] - value).astype(jnp.bfloat16)
+
+
+def out_kernel(ids, x_ref, pooled_ref, *rest, parts, skip):
+    pieces, (r_ref, w_buf, sems) = rest[:parts], rest[parts:]
+    rows, cols = pieces[0].shape[1:]
+    place = lambda target, i, j: target.at[pl.ds(pl.multiple_of(j * rows, rows), rows),
+                                           pl.ds(pl.multiple_of(i * cols, cols), cols)]
+    copies = pieces_at(ids, pieces, w_buf, sems, place)
+    for copy in copies:
+        copy.start()
+    pooled = pooled_ref[:, skip:]
+    for copy in copies:
+        copy.wait()
+    step = 512
+    for start in range(0, w_buf.shape[1], step):
+        change = lax.dot_general(w_buf[:, start:start + step], pooled, contract_rows, preferred_element_type=jnp.float32)
+        own = x_ref[start:start + step, skip:].astype(jnp.float32)
+        r_ref[start:start + step, :] = (own + change).astype(r_ref.dtype)
+
+
+def call(kernel, out, ids, blocks, pieces, scratch):
+    vmem = pl.BlockSpec(memory_space=pltpu.VMEM)
+    return pl.pallas_call(
+        kernel,
+        out_shape=out,
+        in_specs=[pl.BlockSpec(memory_space=pltpu.SMEM)] + [vmem] * len(blocks)
+        + [pl.BlockSpec(memory_space=pl.ANY)] * len(pieces),
+        out_specs=vmem,
+        scratch_shapes=[pltpu.VMEM(scratch, jnp.bfloat16), pltpu.SemaphoreType.DMA((ids.shape[1],))],
+        compiler_params=pltpu.CompilerParams(vmem_limit_bytes=56 * 1024 * 1024),
+    )(ids, *blocks, *pieces)
+
+
+def gathered(block):
+    return [lax.all_gather(block, BOTH)]
+
+
+def gathered_ids():
+    every = lax.iota(jnp.int32, lax.axis_size("sp") * lax.axis_size("tp"))
+    return jnp.stack([every // lax.axis_size("tp"), every % lax.axis_size("tp")])
+
+
+def split_tokens(stream, norm_gain, in_weight, out_weight, docs):
+    length = stream.shape[1]
+    own_len = length // 2
+    half = lax.axis_index("tp")
+    swap = lambda a: lax.ppermute(a, "tp", [(0, 1), (1, 0)])
+    ids = gathered_ids()
+    in_parts = [gathered(in_weight[layer]) for layer in range(LAYERS)]
+    out_parts = [gathered(out_weight[layer]) for layer in range(LAYERS)]
+
+    before = passed_along(stream[:, length - HALO:], "sp", 1)
+    extended = jnp.concatenate([before, stream], axis=1)
+    ext_docs = jnp.concatenate([passed_along(docs[length - HALO:] + 1, "sp", 1), docs + 1])
+    span = own_len + HALO
+    theirs = swap(lax.dynamic_slice_in_dim(extended, (1 - half) * own_len, span, axis=1))
+    ours = lax.dynamic_slice_in_dim(extended, half * own_len, span, axis=1)
+    first = half == 0
+    x = jnp.concatenate([jnp.where(first, ours, theirs), jnp.where(first, theirs, ours)], axis=0)
+    marks = lax.dynamic_slice_in_dim(ext_docs, half * own_len, span)[None, :]
+    gain = lax.all_gather(norm_gain, "tp", axis=1, tiled=True)
+
+    for layer in range(LAYERS):
+        pooled = call(
+            functools.partial(in_kernel, parts=len(in_parts[layer]), layer_first=layer == 0),
+            jax.ShapeDtypeStruct((PW, span), jnp.bfloat16),
+            ids, (x, gain[layer][:, None], marks), in_parts[layer], (D, PW))
+        last = layer == LAYERS - 1
+        skip = HALO if last else 0
+        x = call(
+            functools.partial(out_kernel, parts=len(out_parts[layer]), skip=skip),
+            jax.ShapeDtypeStruct((D, span - skip), jnp.bfloat16 if last else jnp.float32),
+            ids, (x, pooled), out_parts[layer], (PW, D))
+    rows = D // 2
+    kept = lax.dynamic_slice_in_dim(x, half * rows, rows, axis=0)
+    got = swap(lax.dynamic_slice_in_dim(x, (1 - half) * rows, rows, axis=0))
+    return jnp.concatenate([jnp.where(first, kept, got), jnp.where(first, got, kept)], axis=1)
+
+
+def per_device(stream, norm_gain, in_weight, out_weight, docs):
+    tokens_fit = lax.axis_size("tp") == 2 and stream.shape[1] % 256 == 0
+    plan = split_tokens if tokens_fit else split_channels
+    return plan(stream, norm_gain, in_weight, out_weight, docs)
+
+
 def solution(mesh):
     return jax.shard_map(
         per_device,

time: 417 us -> 312 us (0.75)
  blocking collectives: 112 us -> 24.7 us
  Pallas kernels: 0 us -> 40.3 us
  matrix products: 24.4 us -> 0 us
  other arithmetic: 29.6 us -> 6.19 us
  waiting for transfers between devices: 221 us -> 202 us
  starting transfers between devices: 4.9 us -> 11.9 us
    all_to_all x2 -> x0, blocking collectives: 101 us -> none  [per_device(): lax.all_to_all(out_rows, 'tp', split_axis=1, concat_axis=0, tiled=True)]
    all_gather x8 -> x4, waiting for transfers between devices: 219 us -> 175 us  [gathered(): return [lax.all_gather(block, BOTH)]]
    pallas_call x0 -> x4, Pallas kernels: none -> 40.3 us  [call(): pl.pallas_call(kernel, out_shape=out, in_specs=[pl.BlockSpec(memory_space...]
    convert_element_type x7 -> x0, other arithmetic: 27.2 us -> none  [the longest x2 20.8 us: trailing_pool(): (window_sum / members - values.astype(jnp.float32)).astype(jnp.bfloat16)]
    all_gather x0 -> x1, blocking collectives: none -> 24.7 us  [split_tokens(): gain = lax.all_gather(norm_gain, 'tp', axis=1, tiled=True)]
    dot_general x4 -> x0, matrix products: 24.4 us -> none  [the longest x2 13.9 us: per_device(): lax.dot_general(out_cols, lax.all_gather(pooled, 'tp', axis=0, tiled=True...]
    ppermute x0 -> x2, waiting for transfers between devices: none -> 24.1 us  [split_tokens(): swap = lambda a: lax.ppermute(a, 'tp', [(0, 1), (1, 0)])]
    psum x2 -> x0, blocking collectives: 10.8 us -> none  [per_device(): squares = lax.psum(jnp.sum(residual * residual, axis=0), 'tp')]
  transfers between devices with their start and end apart: 11 -> 8, of which waited for: 9 -> 6; matrix products, arithmetic and copies ran while one was open for 13% -> 4% of each run, Pallas kernels for 0% -> 10%
where the time goes in v1:
time: 312 us; the launch traced here: 311 us
  waiting for transfers between devices  202 us (65%)
  Pallas kernels  40.3 us (13%)
  blocking collectives  24.7 us (8%)
  local copies, waits for them, and re-layouts  13.2 us (4%)
  between operations  13.2 us (4%)
  starting transfers between devices  11.9 us (4%)
  other arithmetic  6.19 us (2%)
    all_gather x4, waiting for transfers between devices, gathered(): return [lax.all_gather(block, BOTH)]  175 us
    pallas_call x4, Pallas kernels, call(): pl.pallas_call(kernel, out_shape=out, in_specs=[pl.BlockSpec(memory_space...  40.3 us
    all_gather x1, blocking collectives, split_tokens(): gain = lax.all_gather(norm_gain, 'tp', axis=1, tiled=True)  24.7 us
    ppermute x2, waiting for transfers between devices, split_tokens(): swap = lambda a: lax.ppermute(a, 'tp', [(0, 1), (1, 0)])  24.1 us
    ppermute x2, starting transfers between devices, passed_along(): return lax.ppermute(block, axis, route)  8 us
  transfers between devices with their start and end apart: 8, of which 6 were waited for; matrix products, arithmetic and copies ran while one was open for 4% of the time, Pallas kernels for 10%

profile of v1, /device:TPU:0, one launch (start us, length us, event | category | flops | bytes accessed | tf_op | source)
XLA Modules:
  0.0 311.2 jit_solution(17635251157398201001)
XLA Ops:
  6.5 0.0 all-gather.5.cloned.1.call-start
  6.5 1.7 fusion.2
  8.2 0.0 all-gather.5.cloned.1.call-update
  8.3 0.0 all-gather.7.cloned.1.call-start
  8.3 1.7 fusion.1
  10.1 0.0 all-gather.7.cloned.1.call-update
  10.1 0.0 all-gather.9.cloned.1.call-start
  10.1 0.7 all-gather.9.cloned.1.call-update
  10.8 0.0 all-gather.11.cloned.1.call-start
  10.9 0.5 all-gather.11.cloned.1.call-update
  11.4 1.0 slice.24
  12.4 2.4 collective-permute-start
  14.8 1.1 collective-permute-done
  16.0 1.8 constant_dynamic-update-slice_fusion
  17.7 0.0 copy-start.2
  17.7 0.0 copy-start.1
  17.8 1.2 constant_dynamic-slice_fusion.1
  18.9 2.3 collective-permute-start.1
  21.3 0.0 copy-done.2
  21.3 5.6 %collective-permute-start.2 = (s32[128]{0:T(128)S(1)}, s32[128]{0:T(128)S(1)}, u32[]{:S(2)}, u32[]{:S(2)}) collective-permute-start(s32[128]{0:T(128)S(1)} %slice_add_fusion), channel_id=1, source_target_pairs={{0,2},{2,4},{4,6},{6,8},{8,10},{10,12},{12,14},{14,16},{16,18},{18... | collective-permute-start | bytes 1544 | tf_op jit(solution)/shard_map/ppermute | solution.py:24
  26.9 0.0 copy-done.1
  26.9 24.7 %all_gather.15 = f32[2,2048]{1,0:T(2,128)S(1)} all-gather(f32[2,1024]{1,0:T(2,128)S(1)} %copy-done.1), channel_id=1, replica_groups=mesh['sp'=16,'tp'=2] {'tp'}, dimensions={1}, use_global_device_ids=true | all-gather | bytes 24576 | tf_op jit(solution)/shard_map/all_gather | solution.py:182
  51.6 0.6 pad_add_fusion.ids
  52.2 1.4 copy.8.gain_ref
  53.6 1.4 copy.9.gain_ref
  55.0 0.0 collective-permute-done.2
  55.0 0.1 fusion
  55.0 0.6 broadcast_in_dim.3.docs_ref
  55.6 0.0 collective-permute-done.1
  55.6 1.8 broadcast_select_fusion.1
  57.4 1.7 pad_maximum_fusion.x_ref
  59.1 16.3 %all-gather.5.cloned.1.call-done.rest_0_ = bf16[32,128,512]{2,1,0:T(8,128)(2,1)} async-done(((bf16[1,128,512]{2,1,0:T(8,128)(2,1)}), bf16[32,128,512]{2,1,0:T(8,128)(2,1)}) %all-gather.5.cloned.1.call-update) | async-done | bytes 4194320 | tf_op jit(solution)/shard_map/all_gather | solution.py:156
  75.4 9.9 %shard_map.55.pooled_ref = bf16[1024,640]{1,0:T(8,128)(2,1)} custom-call(s32[2,32]{1,0:T(2,128)} %pad_add_fusion.ids, bf16[2048,640]{1,0:T(8,128)(2,1)} %pad_maximum_fusion.x_ref, f32[2048,1]{1,0:T(8,128)} %copy.8.gain_ref, s32[1,640]{1,0:T(1,128)} %broadcast_in_dim.3.docs_ref, bf16[32,128,512]{2,1,0:T(8,128)(2,1)} %all-gather.5.cloned.1.call-done.rest_0_), custom_call_target="tpu_custom_call" | custom-call | tf_op jit(solution)/shard_map/pallas_call | solution.py:144
  85.3 53.6 %all-gather.7.cloned.1.call-done.rest_0_ = bf16[32,512,128]{2,1,0:T(8,128)(2,1)} async-done(((bf16[1,512,128]{2,1,0:T(8,128)(2,1)}), bf16[32,512,128]{2,1,0:T(8,128)(2,1)}) %all-gather.7.cloned.1.call-update) | async-done | bytes 4194320 | tf_op jit(solution)/shard_map/all_gather | solution.py:156
  138.8 10.5 %shard_map.56.x_ref = f32[2048,640]{1,0:T(8,128)} custom-call(s32[2,32]{1,0:T(2,128)} %pad_add_fusion.ids, bf16[2048,640]{1,0:T(8,128)(2,1)} %pad_maximum_fusion.x_ref, bf16[1024,640]{1,0:T(8,128)(2,1)} %shard_map.55.pooled_ref, bf16[32,512,128]{2,1,0:T(8,128)(2,1)} %all-gather.7.cloned.1.call-done.rest_0_), custom_call_target="tpu_custom_call" | custom-call | tf_op jit(solution)/shard_map/pallas_call | solution.py:144
  149.3 53.0 %all-gather.9.cloned.1.call-done.rest_0_ = bf16[32,128,512]{2,1,0:T(8,128)(2,1)} async-done(((bf16[1,128,512]{2,1,0:T(8,128)(2,1)}), bf16[32,128,512]{2,1,0:T(8,128)(2,1)}) %all-gather.9.cloned.1.call-update) | async-done | bytes 4194320 | tf_op jit(solution)/shard_map/all_gather | solution.py:156
  202.3 10.8 %shard_map.57.pooled_ref = bf16[1024,640]{1,0:T(8,128)(2,1)} custom-call(s32[2,32]{1,0:T(2,128)} %pad_add_fusion.ids, f32[2048,640]{1,0:T(8,128)} %shard_map.56.x_ref, f32[2048,1]{1,0:T(8,128)} %copy.9.gain_ref, s32[1,640]{1,0:T(1,128)} %broadcast_in_dim.3.docs_ref, bf16[32,128,512]{2,1,0:T(8,128)(2,1)} %all-gather.9.cloned.1.call-done.rest_0_), custom_call_target="tpu_custom_call" | custom-call | tf_op jit(solution)/shard_map/pallas_call | solution.py:144
  213.1 52.4 %all-gather.11.cloned.1.call-done.rest_0_ = bf16[32,512,128]{2,1,0:T(8,128)(2,1)} async-done(((bf16[1,512,128]{2,1,0:T(8,128)(2,1)}), bf16[32,512,128]{2,1,0:T(8,128)(2,1)}) %all-gather.11.cloned.1.call-update) | async-done | bytes 4194320 | tf_op jit(solution)/shard_map/all_gather | solution.py:156
  265.6 9.1 %shard_map.58 = bf16[2048,512]{1,0:T(8,128)(2,1)} custom-call(s32[2,32]{1,0:T(2,128)} %pad_add_fusion.ids, f32[2048,640]{1,0:T(8,128)} %shard_map.56.x_ref, bf16[1024,640]{1,0:T(8,128)(2,1)} %shard_map.57.pooled_ref, bf16[32,512,128]{2,1,0:T(8,128)(2,1)} %all-gather.11.cloned.1.call-done.rest_0_), custom_call_target="tpu_custom_call" | custom-call | tf_op jit(solution)/shard_map/pallas_call | solution.py:144
  274.7 0.0 copy-start
  274.7 2.4 constant_dynamic-slice_fusion
  277.1 1.5 collective-permute-start.3
  278.6 24.1 %collective-permute-done.3 = bf16[1024,512]{1,0:T(8,128)(2,1)S(1)} collective-permute-done((bf16[1024,512]{1,0:T(8,128)(2,1)}, bf16[1024,512]{1,0:T(8,128)(2,1)S(1)}, u32[]{:S(2)}, u32[]{:S(2)}) %collective-permute-start.3) | collective-permute-done | bytes 1048608 | tf_op jit(solution)/shard_map/ppermute | solution.py:168
  302.7 0.0 copy-done
  302.7 0.4 broadcast_select_fusion.3
  303.1 1.6 pad_maximum_fusion.1
  (5 shorter events, 0.1 us)
Async XLA Ops:
  6.5 68.9 %all-gather.5.cloned.1.call-start = ((), (), s32[]{:S(2)}) async-start(), calls=%async_computation | async-start | bytes 4325376 | tf_op jit(solution)/shard_map/all_gather | solution.py:156
  8.3 130.6 %all-gather.7.cloned.1.call-start = ((), (), s32[]{:S(2)}) async-start(), calls=%async_computation.1 | async-start | bytes 4325376 | tf_op jit(solution)/shard_map/all_gather | solution.py:156
  10.1 192.2 %all-gather.9.cloned.1.call-start = ((), (), s32[]{:S(2)}) async-start(), calls=%async_computation.2 | async-start | bytes 4325376 | tf_op jit(solution)/shard_map/all_gather | solution.py:156
  10.8 254.7 %all-gather.11.cloned.1.call-start = ((), (), s32[]{:S(2)}) async-start(), calls=%async_computation.3 | async-start | bytes 4325376 | tf_op jit(solution)/shard_map/all_gather | solution.py:156
  12.4 3.5 %collective-permute-start = (bf16[1024,128]{1,0:T(8,128)(2,1)S(1)}, bf16[1024,128]{1,0:T(8,128)(2,1)S(1)}, u32[]{:S(2)}, u32[]{:S(2)}) collective-permute-start(bf16[1024,128]{1,0:T(8,128)(2,1)S(1)} %slice.24), channel_id=1, source_target_pairs={{0,2},{2,4},{4,6},{6,8},{8,10},{10,12},{12,14},{14,16},{16,18},{18... | collective-permute-start | bytes 786440 | tf_op jit(solution)/shard_map/ppermute | solution.py:24
  17.7 3.5 %copy-start.2 = (s32[1024]{0:T(1024)S(1)}, s32[1024]{0:T(1024)}, u32[]{:S(2)}) copy-start(s32[1024]{0:T(1024)} %param.9) | copy-start | bytes 12292
  17.7 9.1 %copy-start.1 = (f32[2,1024]{1,0:T(2,128)S(1)}, f32[2,1024]{1,0:T(2,128)}, u32[]{:S(2)}) copy-start(f32[2,1024]{1,0:T(2,128)} %param.6) | copy-start | bytes 24580
  18.9 36.7 %collective-permute-start.1 = (bf16[1024,640]{1,0:T(8,128)(2,1)}, bf16[1024,640]{1,0:T(8,128)(2,1)}, u32[]{:S(2)}, u32[]{:S(2)}) collective-permute-start(bf16[1024,640]{1,0:T(8,128)(2,1)} %constant_dynamic-slice_fusion.1), channel_id=1, source_target_pairs={{0,1},{1,0},{2,3},{3,2},{4,5},{5,4},{6,7},{7,6},{8,9},{9,8},{10,11... | collective-permute-start | bytes 3932168 | tf_op jit(solution)/shard_map/ppermute | solution.py:168
  21.3 33.7 %collective-permute-start.2 = (s32[128]{0:T(128)S(1)}, s32[128]{0:T(128)S(1)}, u32[]{:S(2)}, u32[]{:S(2)}) collective-permute-start(s32[128]{0:T(128)S(1)} %slice_add_fusion), channel_id=1, source_target_pairs={{0,2},{2,4},{4,6},{6,8},{8,10},{10,12},{12,14},{14,16},{16,18},{18... | collective-permute-start | bytes 1544 | tf_op jit(solution)/shard_map/ppermute | solution.py:24
  274.7 28.0 %copy-start = (bf16[2048,512]{1,0:T(8,128)(2,1)S(1)}, bf16[2048,512]{1,0:T(8,128)(2,1)}, u32[]{:S(2)}) copy-start(bf16[2048,512]{1,0:T(8,128)(2,1)} %shard_map.58) | copy-start | bytes 6291460
  277.1 25.5 %collective-permute-start.3 = (bf16[1024,512]{1,0:T(8,128)(2,1)}, bf16[1024,512]{1,0:T(8,128)(2,1)S(1)}, u32[]{:S(2)}, u32[]{:S(2)}) collective-permute-start(bf16[1024,512]{1,0:T(8,128)(2,1)} %constant_dynamic-slice_fusion), channel_id=1, source_target_pairs={{0,1},{1,0},{2,3},{3,2},{4,5},{5,4},{6,7},{7,6},{8,9},{9,8},{10,11... | collective-permute-start | bytes 3145736 | tf_op jit(solution)/shard_map/ppermute | solution.py:168
Sparse Core Ops, SparseCore 0:
  10.2 65.1 all-gather.4
  78.3 60.4 all-gather.6
  141.7 60.4 all-gather.8
  205.0 60.4 all-gather.10
